TPU v7x, 32 devices: a whole 2x2x4 slice. The times are simulated.
32 devices in a mesh: sp: 4 (over z), fs: 4 (over y, x), tp: 2 (over core).
Axes of the slice: x: 2, y: 2, z: 4, core: 2. Of those that a mesh axis runs over, the one named last changes fastest.
Arguments:
- tokens: bfloat16 [4, 1024, 1024], P('fs', 'sp', 'tp'), may hold values from -6 to 6
- w_inner: bfloat16 [1024, 2048], P('sp', 'tp'), may hold values from -0.1875 to 0.1875
- w_gate: bfloat16 [1024, 2048], P('sp', 'tp'), may hold values from -0.1875 to 0.1875
- w_write: bfloat16 [1024, 512], P('sp', 'tp'), may hold values from -0.1875 to 0.1875
- w_read: bfloat16 [1024, 512], P('sp', 'tp'), may hold values from -0.1875 to 0.1875
- w_pool_in: bfloat16 [1024, 1024], P('sp', 'tp'), may hold values from -0.1875 to 0.1875
- w_step: bfloat16 [1024, 2, 32], replicated, may hold values from -0.1875 to 0.1875
- conv_inner: bfloat16 [5, 2048], replicated, may hold values from -2.5 to 2.5
- conv_cross: bfloat16 [5, 2, 512], replicated, may hold values from -2.5 to 2.5
- rate_log: float32 [2, 32], replicated, may hold values from -20 to -3
- decay_extra: float32 [4, 1024, 2, 32], P('fs', 'sp', None, 'tp'), may hold values from -1 to 0
- norm_gain: float32 [2048], replicated, may hold values from 0.1 to 1.9
- pool_mix: bfloat16 [4, 256, 256], replicated, may hold values from -0.375 to 0.375
- pool_gain: float32 [1024], replicated, may hold values from 0.1 to 1.9
- w_out_inner: bfloat16 [2048, 1024], P('tp', 'fs'), may hold values from -0.109375 to 0.109375
- w_out_pool: bfloat16 [1024, 1024], P('tp', 'fs'), may hold values from -0.109375 to 0.109375
Outputs:
- layer_out: bfloat16 [4, 1024, 1024], P('fs', ('sp', 'tp'))
All inputs are finite; a program needn't handle non-finite values.
Results may differ from a plain program's by a relative error of at most 0.0075.
Values may be sent and summed in bfloat16 or wider, within the bound.
A program may use at most 128 MiB of HBM per device.

v0:
```python
import functools

import jax
import jax.numpy as jnp
from jax import lax
from jax.experimental import pallas as pl
from jax.experimental.pallas import tpu as pltpu
from jax.sharding import PartitionSpec as P

HEAD_DIM = 64
STATE = 128
POOL_DIM = 256
POOL_GROUPS = 4
CONV = 5
GRID_W = 32
EPSILON = 1e-05
HIGHEST = lax.Precision.HIGHEST
MESH = pl.DeviceIdType.MESH
RIM = 16
NH = 2

bf16 = jnp.bfloat16
f32 = jnp.float32


def dot(a, b, precision=None):
    return jnp.dot(a, b, preferred_element_type=f32, precision=precision)


def remote(src, dst, send, recv, axis, target):
    return pltpu.make_async_remote_copy(
        src_ref=src,
        dst_ref=dst,
        send_sem=send,
        recv_sem=recv,
        device_id={axis: target},
        device_id_type=MESH,
    )


def greet(sizes):
    barrier = pltpu.get_barrier_semaphore()
    n_s, n_f, n_t = sizes
    count = 0
    for axis, steps, n in (
        ("sp", (1, n_s - 1), n_s),
        ("fs", range(1, n_f), n_f),
        ("tp", range(1, n_t), n_t),
    ):
        me = lax.axis_index(axis)
        for j in steps:
            pl.semaphore_signal(
                barrier, inc=1, device_id={axis: lax.rem(me + j, n)}, device_id_type=MESH
            )
            count += 1
    pl.semaphore_wait(barrier, count)


def project_kernel(
    sizes, tok, w_inner, w_write, w_read, w_gate, w_pool, w_step,
    out, raw, rim_lo, rim_hi, pool_lo, pool_hi,
    stacked, wg, tg, pbuf,
    up_send, up_recv, dn_send, dn_recv, ft_send, ft_recv, tt_send, tt_recv,
    a_send, a_recv, h_send, h_recv,
):
    n_s, n_f, n_t = sizes
    s, f, t = lax.axis_index("sp"), lax.axis_index("fs"), lax.axis_index("tp")
    rows, half_d = tok.shape
    ks, total = stacked.shape
    share = total // n_f
    hw = share // NH
    stream = rim_lo.shape[1]

    at = 0
    for ref in (w_inner, w_write, w_read, w_gate, w_pool):
        stacked[:, at : at + ref.shape[1]] = ref[...]
        at += ref.shape[1]
    tg[f, t] = tok[...]
    greet(sizes)

    def weight_copy(hh, c, up):
        piece = wg.at[hh, pl.ds(pl.multiple_of(c * ks, ks), ks)]
        if up:
            return remote(piece, piece, up_send.at[hh, c], up_recv.at[hh, c], "sp", s + 1)
        return remote(piece, piece, dn_send.at[hh, c], dn_recv.at[hh, c], "sp", s - 1)

    def column(who, hh):
        return pl.ds(pl.multiple_of(who * share + hh * hw, 128), hw)

    for hh in range(NH):
        wg[hh, pl.ds(pl.multiple_of(s * ks, ks), ks)] = stacked[:, column(f, hh)]

    def relay(hh, k):
        for up in (True, False):
            c = s - k if up else s + k
            inside = c >= 0 if up else c < n_s
            more = s + 1 < n_s if up else s >= 1

            @pl.when(inside)
            def _():
                if k > 0:
                    weight_copy(hh, c, up).wait_recv()

                @pl.when(more)
                def _():
                    weight_copy(hh, c, up).start()

    def tok_fs(j):
        return remote(
            tg.at[f, t], tg.at[f, t], ft_send.at[j], ft_recv.at[j], "fs", lax.rem(f + j, n_f)
        )

    def tok_fs_in(j):
        who = lax.rem(f + n_f - j, n_f)
        return remote(tg.at[who, t], tg.at[who, t], ft_send.at[j], ft_recv.at[j], "fs", who)

    def tok_tp(j, i):
        who = lax.rem(f + n_f - j, n_f)
        to = lax.rem(t + i, n_t)
        return remote(tg.at[who, t], tg.at[who, t], tt_send.at[j, i], tt_recv.at[j, i], "tp", to)

    def tok_tp_in(j, i):
        who = lax.rem(f + n_f - j, n_f)
        src = lax.rem(t + n_t - i, n_t)
        return remote(
            tg.at[who, src], tg.at[who, src], tt_send.at[j, i], tt_recv.at[j, i], "tp", src
        )

    relay(0, 0)
    for j in range(1, n_f):
        tok_fs(j).start()
    for i in range(1, n_t):
        tok_tp(0, i).start()
    for k in range(1, n_s):
        if k == n_s - 1:
            for j in range(1, n_f):
                tok_fs_in(j).wait_recv()
                for i in range(1, n_t):
                    tok_tp(j, i).start()
        relay(0, k)

    def product(who, hh):
        acc = dot(tg[who, 0], wg[hh, 0:half_d])
        for i in range(1, n_t):
            acc = acc + dot(tg[who, i], wg[hh, i * half_d : (i + 1) * half_d])
        return acc.astype(bf16)

    def answer(hh, j):
        return remote(
            pbuf.at[hh, j - 1],
            out.at[:, column(f, hh)],
            a_send.at[hh, j - 1],
            a_recv.at[hh, j - 1],
            "fs",
            lax.rem(f + j, n_f),
        )

    def answer_in(hh, j):
        who = lax.rem(f + n_f - j, n_f)
        return remote(
            pbuf.at[hh, j - 1],
            out.at[:, column(who, hh)],
            a_send.at[hh, j - 1],
            a_recv.at[hh, j - 1],
            "fs",
            who,
        )

    for hh in range(NH):
        if hh + 1 < NH:
            relay(hh + 1, 0)
        if hh == 0:
            for j in range(n_f):
                for i in range(1, n_t):
                    tok_tp_in(j, i).wait_recv()
        for j in range(1, n_f):
            pbuf[hh, j - 1] = product(lax.rem(f + j, n_f), hh)
            answer(hh, j).start()
        out[:, column(f, hh)] = product(f, hh)
        if hh == 0:
            step = dot(tg[f, 0], w_step[0:half_d])
            for i in range(1, n_t):
                step = step + dot(tg[f, i], w_step[i * half_d : (i + 1) * half_d])
            raw[...] = step
        if hh + 1 < NH:
            for k in range(1, n_s):
                relay(hh + 1, k)

    for hh in range(NH):
        for j in range(1, n_f):
            answer_in(hh, j).wait_recv()

    pool_at = total - pool_lo.shape[1]
    halo = (
        (out.at[rows - RIM : rows, 0:stream], rim_lo, 0, True),
        (out.at[:, pool_at:total], pool_lo, 1, True),
        (out.at[0:RIM, 0:stream], rim_hi, 2, False),
        (out.at[:, pool_at:total], pool_hi, 3, False),
    )

    def halo_copy(item):
        src, dst, sem, up = item
        return remote(src, dst, h_send.at[sem], h_recv.at[sem], "sp", s + 1 if up else s - 1)

    for item in halo:
        up = item[3]

        @pl.when(s + 1 < n_s if up else s >= 1)
        def _():
            halo_copy(item).start()

        @pl.when(s == 0 if up else s == n_s - 1)
        def _():
            item[1][...] = jnp.zeros_like(item[1])

    for hh in range(NH):
        for k in range(n_s):
            for up in (True, False):
                c = s - k if up else s + k

                @pl.when(
                    jnp.logical_and(c >= 0, s + 1 < n_s)
                    if up
                    else jnp.logical_and(c < n_s, s >= 1)
                )
                def _():
                    weight_copy(hh, c, up).wait_send()

        for j in range(1, n_f):
            answer(hh, j).wait_send()
    for j in range(n_f):
        if j > 0:
            tok_fs(j).wait_send()
        for i in range(1, n_t):
            tok_tp(j, i).wait_send()
    for item in halo:
        up = item[3]

        @pl.when(s >= 1 if up else s + 1 < n_s)
        def _():
            halo_copy(item).wait_recv()

        @pl.when(s + 1 < n_s if up else s >= 1)
        def _():
            halo_copy(item).wait_send()


def mixer_kernel(
    sizes, proj, raw, rim_lo, rim_hi, pool_lo, pool_hi, extra, rate_log, taps, norm_gain,
    mix, pool_gain, wo_inner, wo_pool,
    result,
    frame, act, inside, wo_i, wo_p, sum_f, sum_b, out_f, out_b, in_f, in_b, part, peer, pooled,
    o_send, o_recv, f_send, f_recv, b_send, b_recv, t_send, t_recv,
):
    n_s, n_f, n_t = sizes
    s, f, t = lax.axis_index("sp"), lax.axis_index("fs"), lax.axis_index("tp")
    rows = proj.shape[0]
    stream = rim_lo.shape[1]
    inner = norm_gain.shape[1]
    heads = inner // HEAD_DIM
    cross = (stream - inner) // 2
    groups = cross // STATE
    per = heads // groups
    wide = per * HEAD_DIM
    greet(sizes)

    def out_copy(j, who, n):
        src, dst = ((wo_inner, wo_i), (wo_pool, wo_p))[n]
        return remote(
            src, dst.at[who], o_send.at[j, n], o_recv.at[j, n], "fs", lax.rem(f + j, n_f)
        )

    for j in range(1, n_f):
        for n in range(2):
            out_copy(j, f, n).start()
    wo_i[f] = wo_inner[...]
    wo_p[f] = wo_pool[...]

    step = jax.nn.softplus(raw[...])
    decay = extra[...] - step * jnp.exp(rate_log[...])
    row_id = lax.broadcasted_iota(jnp.int32, (rows, rows), 0)
    col_id = lax.broadcasted_iota(jnp.int32, (rows, rows), 1)
    lower = (row_id >= col_id).astype(f32)
    upper = (row_id <= col_id).astype(f32)
    run_f = dot(lower, decay[:, :heads], HIGHEST)
    run_b = dot(upper, decay[:, heads:], HIGHEST)
    last_f, last_b = run_f[rows - 1 : rows], run_b[0:1]
    spread_r = lax.broadcasted_iota(jnp.int32, (2 * heads, inner), 0)
    spread_c = lax.broadcasted_iota(jnp.int32, (2 * heads, inner), 1)
    spread_m = (lax.rem(spread_r, heads) == spread_c // HEAD_DIM).astype(bf16)
    gather_r = lax.broadcasted_iota(jnp.int32, (inner, heads), 0)
    gather_c = lax.broadcasted_iota(jnp.int32, (inner, heads), 1)
    gather_m = (gather_r // HEAD_DIM == gather_c).astype(bf16)

    def split(x):
        high = x.astype(bf16)
        return high, (x - high.astype(f32)).astype(bf16)

    def spread(x):
        return dot(jnp.concatenate(split(x), axis=1), spread_m)

    frame[0:8] = rim_lo[RIM - 8 : RIM].astype(f32)
    frame[8 : 8 + rows] = proj[:, :stream].astype(f32)
    frame[8 + rows : 16 + rows] = rim_hi[0:8].astype(f32)
    first = 8 - CONV // 2
    total = frame[first : first + rows] * taps[0:1]
    for k in range(1, CONV):
        total = total + frame[first + k : first + k + rows] * taps[k : k + 1]
    act[...] = (total * jax.nn.sigmoid(total)).astype(bf16)

    def cut(kind, g):
        at = inner + kind * cross + g * STATE
        return act[:, at : at + STATE]

    tail_f = spread(jnp.exp(last_f - run_f) * step[:, :heads])
    tail_b = spread(jnp.exp(last_b - run_b) * step[:, heads:])
    ones = jnp.ones((8, 1), f32)
    keep_f = spread(jnp.exp(last_f) * ones)[0:1]
    keep_b = spread(jnp.exp(last_b) * ones)[0:1]

    def chain_copy(forward, g):
        src, dst, send, recv = (
            (out_f, in_f, f_send, f_recv) if forward else (out_b, in_b, b_send, b_recv)
        )
        return remote(
            src.at[g], dst.at[g], send.at[g], recv.at[g], "sp", s + 1 if forward else s - 1
        )

    for g in range(groups):
        cols = slice(g * wide, (g + 1) * wide)
        vals = act[:, cols].astype(f32)
        writes = cut(0, g).T
        sum_f[g] = dot(writes, (vals * tail_f[:, cols]).astype(bf16))
        sum_b[g] = dot(writes, (vals * tail_b[:, cols]).astype(bf16))

        @pl.when(s == 0)
        def _():
            in_f[g] = jnp.zeros_like(in_f[g])
            out_f[g] = sum_f[g].astype(bf16)
            chain_copy(True, g).start()

        @pl.when(s == n_s - 1)
        def _():
            in_b[g] = jnp.zeros_like(in_b[g])
            out_b[g] = sum_b[g].astype(bf16)
            chain_copy(False, g).start()

    def hand_on(d):
        @pl.when(s == d)
        def _():
            for g in range(groups):
                chain_copy(True, g).wait_recv()
                if d < n_s - 1:
                    cols = slice(g * wide, (g + 1) * wide)
                    out_f[g] = (in_f[g].astype(f32) * keep_f[:, cols] + sum_f[g]).astype(bf16)
                    chain_copy(True, g).start()

        @pl.when(s == n_s - 1 - d)
        def _():
            for g in range(groups):
                chain_copy(False, g).wait_recv()
                if d < n_s - 1:
                    cols = slice(g * wide, (g + 1) * wide)
                    out_b[g] = (in_b[g].astype(f32) * keep_b[:, cols] + sum_b[g]).astype(bf16)
                    chain_copy(False, g).start()

    after = row_id > col_id
    same = row_id == col_id
    side = jnp.concatenate([run_f, run_b, step], axis=1).T

    def head_part(g):
        def work():
            scores = lax.dot_general(
                cut(1, g), cut(0, g), (((1,), (1,)), ((), ())), preferred_element_type=f32
            )
            for h in range(g * per, (g + 1) * per, 2):
                pair = []
                for a in (h, h + 1):
                    fwd = run_f[:, a : a + 1] - side[a : a + 1]
                    bwd = run_b[:, a : a + 1] - side[heads + a : heads + a + 1]
                    dt_f = side[2 * heads + a : 2 * heads + a + 1]
                    dt_b = side[3 * heads + a : 3 * heads + a + 1]
                    scale = jnp.where(after, dt_f, dt_b) + jnp.where(same, dt_f, 0.0)
                    weight = scores * jnp.exp(jnp.where(after, fwd, bwd)) * scale
                    value = act[:, a * HEAD_DIM : (a + 1) * HEAD_DIM]
                    pair.append(dot(weight.astype(bf16), value))
                inside[:, h * HEAD_DIM : (h + 2) * HEAD_DIM] = jnp.concatenate(pair, axis=1)

        return work

    def pool_part():
        grid_rows = rows // GRID_W
        pool_at = proj.shape[1] - pooled.shape[1]
        here = pooled.shape[1] // POOL_DIM
        r, c = row_id // GRID_W, lax.rem(row_id, GRID_W)
        rj, cj = col_id // GRID_W, lax.rem(col_id, GRID_W)
        one = lax.broadcasted_iota(jnp.int32, (rows, 1), 0)
        r1, c1 = one // GRID_W + s * grid_rows, lax.rem(one, GRID_W)
        for slot in range(here):
            reach = jnp.left_shift(jnp.int32(1), t * here + slot)
            cols = slice(slot * POOL_DIM, (slot + 1) * POOL_DIM)
            col_in = jnp.logical_and(cj - c >= -reach, cj - c < reach)
            box = jnp.zeros((rows, POOL_DIM), f32)
            own = proj[:, pool_at + slot * POOL_DIM : pool_at + (slot + 1) * POOL_DIM]
            for shift, source in (
                (-grid_rows, pool_lo[:, cols]),
                (0, own),
                (grid_rows, pool_hi[:, cols]),
            ):
                gap = rj + shift - r
                mask = jnp.logical_and(jnp.logical_and(gap >= -reach, gap < reach), col_in)
                box = box + dot(mask.astype(f32).astype(bf16), source)
            high_r = jnp.minimum(r1 + reach, n_s * grid_rows)
            n_rows = high_r - jnp.maximum(r1 - reach, 0)
            n_cols = jnp.minimum(c1 + reach, GRID_W) - jnp.maximum(c1 - reach, 0)
            average = box / (n_rows * n_cols).astype(f32)
            offsets = (average - own.astype(f32)).astype(bf16)
            pooled[:, cols] = (dot(offsets, mix[slot]) * pool_gain[:, cols]).astype(bf16)

    works = [head_part(g) for g in range(groups)] + [pool_part]
    for d in range(1, n_s):
        if works:
            works.pop(0)()
        hand_on(d)
    while works:
        works.pop(0)()

    lead_f, lead_b = spread(jnp.exp(run_f)), spread(jnp.exp(run_b))
    for g in range(groups):
        cols = slice(g * wide, (g + 1) * wide)
        reads = cut(1, g)
        mixed = inside[:, cols] + dot(reads, in_f[g]) * lead_f[:, cols]
        mixed = mixed + dot(reads, in_b[g]) * lead_b[:, cols]
        gate = proj[:, stream + g * wide : stream + (g + 1) * wide].astype(f32)
        inside[:, cols] = mixed * (gate * jax.nn.sigmoid(gate))
    gated = inside[...]
    high, low = split(gated * gated)
    mean = (dot(high, gather_m) + dot(low, gather_m)) * (1.0 / HEAD_DIM)
    scale = spread(lax.rsqrt(mean + EPSILON))
    mixer = (gated * scale * norm_gain[...]).astype(bf16)

    for j in range(1, n_f):
        for n in range(2):
            out_copy(j, lax.rem(f + n_f - j, n_f), n).wait_recv()
    width = wo_inner.shape[1]
    for w in range(n_f):
        part[:, w * width : (w + 1) * width] = (
            dot(mixer, wo_i[w]) + dot(pooled[...], wo_p[w])
        ).astype(bf16)

    keep = rows // n_t

    def part_of(who):
        return pl.ds(pl.multiple_of(who * keep, keep), keep)

    def last_copy(i):
        to = lax.rem(t + i, n_t)
        return remote(
            part.at[part_of(to)], peer.at[i - 1], t_send.at[i - 1], t_recv.at[i - 1], "tp", to
        )

    for i in range(1, n_t):
        last_copy(i).start()
    for j in range(1, n_f):
        for n in range(2):
            out_copy(j, f, n).wait_send()
    for g in range(groups):

        @pl.when(s + 1 < n_s)
        def _():
            chain_copy(True, g).wait_send()

        @pl.when(s >= 1)
        def _():
            chain_copy(False, g).wait_send()

    acc = part[part_of(t)].astype(f32)
    for i in range(1, n_t):
        last_copy(i).wait_recv()
        acc = acc + peer[i - 1].astype(f32)
    result[...] = acc.astype(bf16)
    for i in range(1, n_t):
        last_copy(i).wait_send()


def body(
    sizes, tokens, w_inner, w_gate, w_write, w_read, w_pool_in, w_step, conv_inner, conv_cross,
    rate_log, decay_extra, norm_gain, pool_mix, pool_gain, w_out_inner, w_out_pool,
):
    n_s, n_f, n_t = sizes
    tp_rank = lax.axis_index("tp")
    tok = tokens[0]
    rows, half_d = tok.shape
    ks, inner = w_inner.shape
    cross = w_write.shape[1]
    pool = w_pool_in.shape[1]
    heads = inner // HEAD_DIM
    groups = cross // STATE
    stream = inner + 2 * cross
    total = stream + inner + pool
    hw = total // n_f // NH
    d = half_d * n_t

    def mine(array, axis):
        size = array.shape[axis] // n_t
        return lax.dynamic_slice_in_dim(array, tp_rank * size, size, axis)

    step_w = mine(w_step, 2).reshape(d, 2 * heads)
    taps = jnp.concatenate(
        [mine(conv_inner, 1), mine(conv_cross[:, 0], 1), mine(conv_cross[:, 1], 1)], axis=1
    ).astype(f32)
    vmem = pl.BlockSpec(memory_space=pltpu.VMEM)
    dma = pltpu.SemaphoreType.DMA

    def shape(*dims, kind=bf16):
        return jax.ShapeDtypeStruct(dims, kind)

    moved = pl.pallas_call(
        functools.partial(project_kernel, sizes),
        out_shape=(
            shape(rows, total),
            shape(rows, 2 * heads, kind=f32),
            shape(RIM, stream),
            shape(RIM, stream),
            shape(rows, pool),
            shape(rows, pool),
        ),
        in_specs=[vmem] * 7,
        out_specs=(vmem,) * 6,
        scratch_shapes=[
            pltpu.VMEM((ks, total), bf16),
            pltpu.VMEM((NH, d, hw), bf16),
            pltpu.VMEM((n_f, n_t, rows, half_d), bf16),
            pltpu.VMEM((NH, n_f - 1, rows, hw), bf16),
            dma((NH, n_s)), dma((NH, n_s)), dma((NH, n_s)), dma((NH, n_s)),
            dma((n_f,)), dma((n_f,)), dma((n_f, n_t)), dma((n_f, n_t)),
            dma((NH, n_f - 1)), dma((NH, n_f - 1)), dma((4,)), dma((4,)),
        ],
        compiler_params=pltpu.CompilerParams(collective_id=0, has_side_effects=True),
    )(tok, w_inner, w_write, w_read, w_gate, w_pool_in, step_w)

    result = pl.pallas_call(
        functools.partial(mixer_kernel, sizes),
        out_shape=shape(rows // n_t, d),
        in_specs=[vmem] * 14,
        out_specs=vmem,
        scratch_shapes=[
            pltpu.VMEM((rows + 16, stream), f32),
            pltpu.VMEM((rows, stream), bf16),
            pltpu.VMEM((rows, inner), f32),
            pltpu.VMEM((n_f,) + w_out_inner.shape, bf16),
            pltpu.VMEM((n_f,) + w_out_pool.shape, bf16),
            pltpu.VMEM((groups, STATE, inner // groups), f32),
            pltpu.VMEM((groups, STATE, inner // groups), f32),
            pltpu.VMEM((groups, STATE, inner // groups), bf16),
            pltpu.VMEM((groups, STATE, inner // groups), bf16),
            pltpu.VMEM((groups, STATE, inner // groups), bf16),
            pltpu.VMEM((groups, STATE, inner // groups), bf16),
            pltpu.VMEM((rows, d), bf16),
            pltpu.VMEM((n_t - 1, rows // n_t, d), bf16),
            pltpu.VMEM((rows, pool), bf16),
            dma((n_f, 2)), dma((n_f, 2)), dma((groups,)), dma((groups,)),
            dma((groups,)), dma((groups,)), dma((n_t - 1,)), dma((n_t - 1,)),
        ],
        compiler_params=pltpu.CompilerParams(collective_id=1, has_side_effects=True),
    )(
        *moved,
        decay_extra[0].reshape(rows, 2 * heads),
        mine(rate_log, 1).reshape(1, 2 * heads),
        taps,
        mine(norm_gain, 0)[None],
        mine(pool_mix, 0),
        mine(pool_gain, 0)[None],
        w_out_inner,
        w_out_pool,
    )
    return result[None]


def solution(mesh):
    sizes = tuple(mesh.shape[axis] for axis in ("sp", "fs", "tp"))
    return jax.shard_map(
        functools.partial(body, sizes),
        mesh=mesh,
        in_specs=(
            P("fs", "sp", "tp"),
            P("sp", "tp"),
            P("sp", "tp"),
            P("sp", "tp"),
            P("sp", "tp"),
            P("sp", "tp"),
            P(),
            P(),
            P(),
            P(),
            P("fs", "sp", None, "tp"),
            P(),
            P(),
            P(),
            P("tp", "fs"),
            P("tp", "fs"),
        ),
        out_specs=P("fs", ("sp", "tp"), None),
        check_vma=False,
    )
```

profile of v0, /device:TPU:9, one launch (start us, length us, event | category | flops | bytes accessed | tf_op | source)
XLA Modules:
  0.0 105.4 jit_solution(8780197323954296855)
XLA Ops:
  0.0 0.0 copy-start
  0.0 0.0 copy-start.2
  0.0 0.0 copy-start.4
  0.0 0.8 fusion
  0.9 0.7 constant_dynamic-slice_fusion.3
  1.6 0.6 maximum_convert_fusion.taps
  2.2 0.0 copy-start.3
  2.2 0.0 copy-start.1
  2.2 0.9 constant_dynamic-slice_fusion.5
  3.1 0.8 copy.19.w_step
  3.9 46.0 %shard_map.154 = (bf16[256,3072]{1,0:T(8,128)(2,1)}, f32[256,32]{1,0:T(8,128)}, bf16[16,1536]{1,0:T(8,128)(2,1)}, bf16[16,1536]{1,0:T(8,128)(2,1)}, bf16[256,512]{1,0:T(8,128)(2,1)}, /*index=5*/bf16[256,512]{1,0:T(8,128)(2,1)}) custom-call(bf16[256,512]{1,0:T(8,128)(2,1)} %bitcast.14, bf16[256,1024]{1,0:T(8,128)(2,1)} %w_inner.1, bf16[256,256]{1,0:T(8,128)(2,1)} %w_write.1, ...), custom_call_target="tpu_custom_call" | custom-call | tf_op jit(solution)/shard_map/pallas_call | solution.py:518
  49.9 0.0 copy-done.2
  49.9 0.6 dynamic_slice.35
  50.5 0.0 copy-done.4
  50.5 0.1 constant_dynamic-slice_fusion.4
  50.6 0.6 reshape.9.rate_log
  51.2 0.0 copy-done
  51.2 0.7 constant_dynamic-slice_fusion.mix
  52.0 0.0 copy-done.3
  52.0 0.7 dynamic_slice.37
  52.6 0.0 copy-done.1
  52.6 0.7 copy.22.extra
  53.4 50.4 %shard_map.155 = bf16[128,1024]{1,0:T(8,128)(2,1)} custom-call(bf16[256,3072]{1,0:T(8,128)(2,1)} %get-tuple-element.11.proj, f32[256,32]{1,0:T(8,128)} %get-tuple-element.12.raw, bf16[16,1536]{1,0:T(8,128)(2,1)} %get-tuple-element.13.rim_lo, bf16[16,1536]{1,0:T(8,128)(2,1)} %get-tuple-element.14.rim_hi, bf16[256,512]{1,0:T(8,128)(2,1)} %get-tuple-element.15.pool_lo, ...), custom_call_target="tpu_custom_call" | custom-call | tf_op jit(solution)/shard_map/pallas_call | solution.py:542
  103.7 1.7 %copy.32 = bf16[1,128,1024]{2,1,0:T(8,128)(2,1)} copy(bf16[1,128,1024]{2,1,0:T(8,128)(2,1)} %bitcast.12) | data formatting | bytes 524288
  (3 shorter events, 0.0 us)
Async XLA Ops:
  0.0 51.2 %copy-start = (bf16[4,256,256]{2,1,0:T(8,128)(2,1)S(1)}, bf16[4,256,256]{2,1,0:T(8,128)(2,1)}, u32[]{:S(2)}) copy-start(bf16[4,256,256]{2,1,0:T(8,128)(2,1)} %param.28) | copy-start | bytes 1572868
  0.0 49.9 %copy-start.2 = (f32[2048]{0:T(1024)S(1)}, f32[2048]{0:T(1024)}, u32[]{:S(2)}) copy-start(f32[2048]{0:T(1024)} %param.27) | copy-start | bytes 24580
  0.0 50.5 %copy-start.4 = (f32[2,32]{1,0:T(2,128)S(1)}, f32[2,32]{1,0:T(2,128)}, u32[]{:S(2)}) copy-start(f32[2,32]{1,0:T(2,128)} %param.25) | copy-start | bytes 772
  2.2 49.7 %copy-start.3 = (f32[1024]{0:T(1024)S(1)}, f32[1024]{0:T(1024)}, u32[]{:S(2)}) copy-start(f32[1024]{0:T(1024)} %param.29) | copy-start | bytes 12292
  2.2 50.4 %copy-start.1 = (f32[1,256,2,16]{1,3,2,0:T(8,128)S(1)}, f32[1,256,2,16]{1,3,2,0:T(8,128)}, u32[]{:S(2)}) copy-start(f32[1,256,2,16]{1,3,2,0:T(8,128)} %param.26) | copy-start | bytes 98308
where the time goes:
time: 106 us; the launch traced here: 105 us
  Pallas kernels  96.4 us (91%)
  local copies, waits for them, and re-layouts  8.34 us (8%)
    pallas_call x1, Pallas kernels, body(): pl.pallas_call(functools.partial(mixer_kernel, sizes), out_shape=shape(ro...  50.4 us
    pallas_call x1, Pallas kernels, body(): pl.pallas_call(functools.partial(project_kernel, sizes), out_shape=(shape...  46 us
    dynamic_slice x7, local copies, waits for them, and re-layouts, mine(): return lax.dynamic_slice_in_dim(array, tp_rank * size, size, axis)  3.65 us

commit v1 on v0

--- a/solution.py
+++ b/solution.py
@@ -36,6 +36,13 @@
         device_id={axis: target},
         device_id_type=MESH,
     )
+
+
+def pick(array, t, n_t, size, at):
+    mine = array[:, at : at + size]
+    for i in range(1, n_t):
+        mine = jnp.where(t == i, array[:, at + i * size : at + (i + 1) * size], mine)
+    return mine
 
 
 def greet(sizes):
@@ -57,11 +64,11 @@
 
 
 def project_kernel(
-    sizes, tok, w_inner, w_write, w_read, w_gate, w_pool, w_step,
-    out, raw, rim_lo, rim_hi, pool_lo, pool_hi,
+    sizes, tok, w_inner, w_write, w_read, w_gate, w_pool, w_step, wo_pool,
+    out, raw, rim_lo, rim_hi, pool_lo, pool_hi, wo_p,
     stacked, wg, tg, pbuf,
     up_send, up_recv, dn_send, dn_recv, ft_send, ft_recv, tt_send, tt_recv,
-    a_send, a_recv, h_send, h_recv,
+    a_send, a_recv, h_send, h_recv, o_send, o_recv,
 ):
     n_s, n_f, n_t = sizes
     s, f, t = lax.axis_index("sp"), lax.axis_index("fs"), lax.axis_index("tp")
@@ -70,9 +77,10 @@
     share = total // n_f
     hw = share // NH
     stream = rim_lo.shape[1]
+    pool_half = (pool_lo.shape[1] - 1) // (n_f * hw)
 
     at = 0
-    for ref in (w_inner, w_write, w_read, w_gate, w_pool):
+    for ref in (w_pool, w_gate, w_inner, w_write, w_read):
         stacked[:, at : at + ref.shape[1]] = ref[...]
         at += ref.shape[1]
     tg[f, t] = tok[...]
@@ -85,7 +93,7 @@
         return remote(piece, piece, dn_send.at[hh, c], dn_recv.at[hh, c], "sp", s - 1)
 
     def column(who, hh):
-        return pl.ds(pl.multiple_of(who * share + hh * hw, 128), hw)
+        return pl.ds(pl.multiple_of((hh * n_f + who) * hw, 128), hw)
 
     for hh in range(NH):
         wg[hh, pl.ds(pl.multiple_of(s * ks, ks), ks)] = stacked[:, column(f, hh)]
@@ -126,11 +134,18 @@
             tg.at[who, src], tg.at[who, src], tt_send.at[j, i], tt_recv.at[j, i], "tp", src
         )
 
+    def out_copy(j, who):
+        to = lax.rem(f + j, n_f)
+        return remote(wo_pool, wo_p.at[who], o_send.at[j], o_recv.at[j], "fs", to)
+
     relay(0, 0)
     for j in range(1, n_f):
         tok_fs(j).start()
+    for j in range(1, n_f):
+        out_copy(j, f).start()
     for i in range(1, n_t):
         tok_tp(0, i).start()
+    wo_p[f] = wo_pool[...]
     for k in range(1, n_s):
         if k == n_s - 1:
             for j in range(1, n_f):
@@ -181,37 +196,44 @@
             step = dot(tg[f, 0], w_step[0:half_d])
             for i in range(1, n_t):
                 step = step + dot(tg[f, i], w_step[i * half_d : (i + 1) * half_d])
-            raw[...] = step
+            heads = raw.shape[1] // 2
+            raw[:, :heads] = pick(step, t, n_t, heads, 0)
+            raw[:, heads:] = pick(step, t, n_t, heads, heads * n_t)
         if hh + 1 < NH:
             for k in range(1, n_s):
                 relay(hh + 1, k)
 
+    pool = pool_lo.shape[1]
+    stream_at = total - stream
+    halo = (
+        (out.at[:, 0:pool], pool_lo, 0, True),
+        (out.at[:, 0:pool], pool_hi, 1, False),
+        (out.at[rows - RIM : rows, stream_at:total], rim_lo, 2, True),
+        (out.at[0:RIM, stream_at:total], rim_hi, 3, False),
+    )
+
+    def halo_copy(item):
+        src, dst, sem, up = item
+        return remote(src, dst, h_send.at[sem], h_recv.at[sem], "sp", s + 1 if up else s - 1)
+
+    def start_halo(items):
+        for item in items:
+            up = item[3]
+
+            @pl.when(s + 1 < n_s if up else s >= 1)
+            def _():
+                halo_copy(item).start()
+
+            @pl.when(s == 0 if up else s == n_s - 1)
+            def _():
+                item[1][...] = jnp.zeros_like(item[1])
+
     for hh in range(NH):
         for j in range(1, n_f):
             answer_in(hh, j).wait_recv()
-
-    pool_at = total - pool_lo.shape[1]
-    halo = (
-        (out.at[rows - RIM : rows, 0:stream], rim_lo, 0, True),
-        (out.at[:, pool_at:total], pool_lo, 1, True),
-        (out.at[0:RIM, 0:stream], rim_hi, 2, False),
-        (out.at[:, pool_at:total], pool_hi, 3, False),
-    )
-
-    def halo_copy(item):
-        src, dst, sem, up = item
-        return remote(src, dst, h_send.at[sem], h_recv.at[sem], "sp", s + 1 if up else s - 1)
-
-    for item in halo:
-        up = item[3]
-
-        @pl.when(s + 1 < n_s if up else s >= 1)
-        def _():
-            halo_copy(item).start()
-
-        @pl.when(s == 0 if up else s == n_s - 1)
-        def _():
-            item[1][...] = jnp.zeros_like(item[1])
+        if hh == pool_half:
+            start_halo(halo[:2])
+    start_halo(halo[2:])
 
     for hh in range(NH):
         for k in range(n_s):
@@ -231,6 +253,8 @@
     for j in range(n_f):
         if j > 0:
             tok_fs(j).wait_send()
+            out_copy(j, f).wait_send()
+            out_copy(j, lax.rem(f + n_f - j, n_f)).wait_recv()
         for i in range(1, n_t):
             tok_tp(j, i).wait_send()
     for item in halo:
@@ -246,17 +270,19 @@
 
 
 def mixer_kernel(
-    sizes, proj, raw, rim_lo, rim_hi, pool_lo, pool_hi, extra, rate_log, taps, norm_gain,
-    mix, pool_gain, wo_inner, wo_pool,
+    sizes, proj, raw, rim_lo, rim_hi, pool_lo, pool_hi, wo_p, extra, rate_log, conv_inner,
+    conv_cross, norm_gain, mix, pool_gain, wo_inner,
     result,
-    frame, act, inside, wo_i, wo_p, sum_f, sum_b, out_f, out_b, in_f, in_b, part, peer, pooled,
+    frame, act, inside, wo_i, sum_f, sum_b, out_f, out_b, in_f, in_b, part, peer, pooled,
     o_send, o_recv, f_send, f_recv, b_send, b_recv, t_send, t_recv,
 ):
     n_s, n_f, n_t = sizes
     s, f, t = lax.axis_index("sp"), lax.axis_index("fs"), lax.axis_index("tp")
     rows = proj.shape[0]
     stream = rim_lo.shape[1]
-    inner = norm_gain.shape[1]
+    inner = norm_gain.shape[1] // n_t
+    stream_at = proj.shape[1] - stream
+    gate_at = stream_at - inner
     heads = inner // HEAD_DIM
     cross = (stream - inner) // 2
     groups = cross // STATE
@@ -264,20 +290,21 @@
     wide = per * HEAD_DIM
     greet(sizes)
 
-    def out_copy(j, who, n):
-        src, dst = ((wo_inner, wo_i), (wo_pool, wo_p))[n]
-        return remote(
-            src, dst.at[who], o_send.at[j, n], o_recv.at[j, n], "fs", lax.rem(f + j, n_f)
-        )
+    def out_copy(j, who):
+        to = lax.rem(f + j, n_f)
+        return remote(wo_inner, wo_i.at[who], o_send.at[j], o_recv.at[j], "fs", to)
 
     for j in range(1, n_f):
-        for n in range(2):
-            out_copy(j, f, n).start()
+        out_copy(j, f).start()
     wo_i[f] = wo_inner[...]
-    wo_p[f] = wo_pool[...]
+
+    def own(ref, size, at=0):
+        return ref[:, pl.ds(pl.multiple_of(at + t * size, 128), size)].astype(f32)
 
     step = jax.nn.softplus(raw[...])
-    decay = extra[...] - step * jnp.exp(rate_log[...])
+    rates = jnp.exp(rate_log[...])
+    rates = [pick(rates[k : k + 1], t, n_t, heads, 0) for k in (0, 1)]
+    decay = extra[...] - step * jnp.concatenate(rates, axis=1)
     row_id = lax.broadcasted_iota(jnp.int32, (rows, rows), 0)
     col_id = lax.broadcasted_iota(jnp.int32, (rows, rows), 1)
     lower = (row_id >= col_id).astype(f32)
@@ -300,8 +327,12 @@
         return dot(jnp.concatenate(split(x), axis=1), spread_m)
 
     frame[0:8] = rim_lo[RIM - 8 : RIM].astype(f32)
-    frame[8 : 8 + rows] = proj[:, :stream].astype(f32)
+    frame[8 : 8 + rows] = proj[:, stream_at:].astype(f32)
     frame[8 + rows : 16 + rows] = rim_hi[0:8].astype(f32)
+    taps = jnp.concatenate(
+        [own(conv_inner, inner), own(conv_cross, cross), own(conv_cross, cross, cross * n_t)],
+        axis=1,
+    )
     first = 8 - CONV // 2
     total = frame[first : first + rows] * taps[0:1]
     for k in range(1, CONV):
@@ -390,7 +421,7 @@
 
     def pool_part():
         grid_rows = rows // GRID_W
-        pool_at = proj.shape[1] - pooled.shape[1]
+        gains = own(pool_gain, pooled.shape[1])
         here = pooled.shape[1] // POOL_DIM
         r, c = row_id // GRID_W, lax.rem(row_id, GRID_W)
         rj, cj = col_id // GRID_W, lax.rem(col_id, GRID_W)
@@ -401,10 +432,10 @@
             cols = slice(slot * POOL_DIM, (slot + 1) * POOL_DIM)
             col_in = jnp.logical_and(cj - c >= -reach, cj - c < reach)
             box = jnp.zeros((rows, POOL_DIM), f32)
-            own = proj[:, pool_at + slot * POOL_DIM : pool_at + (slot + 1) * POOL_DIM]
+            centre = proj[:, cols]
             for shift, source in (
                 (-grid_rows, pool_lo[:, cols]),
-                (0, own),
+                (0, centre),
                 (grid_rows, pool_hi[:, cols]),
             ):
                 gap = rj + shift - r
@@ -414,8 +445,8 @@
             n_rows = high_r - jnp.maximum(r1 - reach, 0)
             n_cols = jnp.minimum(c1 + reach, GRID_W) - jnp.maximum(c1 - reach, 0)
             average = box / (n_rows * n_cols).astype(f32)
-            offsets = (average - own.astype(f32)).astype(bf16)
-            pooled[:, cols] = (dot(offsets, mix[slot]) * pool_gain[:, cols]).astype(bf16)
+            offsets = (average - centre.astype(f32)).astype(bf16)
+            pooled[:, cols] = (dot(offsets, mix[t * here + slot]) * gains[:, cols]).astype(bf16)
 
     works = [head_part(g) for g in range(groups)] + [pool_part]
     for d in range(1, n_s):
@@ -431,17 +462,16 @@
         reads = cut(1, g)
         mixed = inside[:, cols] + dot(reads, in_f[g]) * lead_f[:, cols]
         mixed = mixed + dot(reads, in_b[g]) * lead_b[:, cols]
-        gate = proj[:, stream + g * wide : stream + (g + 1) * wide].astype(f32)
+        gate = proj[:, gate_at + g * wide : gate_at + (g + 1) * wide].astype(f32)
         inside[:, cols] = mixed * (gate * jax.nn.sigmoid(gate))
     gated = inside[...]
     high, low = split(gated * gated)
     mean = (dot(high, gather_m) + dot(low, gather_m)) * (1.0 / HEAD_DIM)
     scale = spread(lax.rsqrt(mean + EPSILON))
-    mixer = (gated * scale * norm_gain[...]).astype(bf16)
+    mixer = (gated * scale * own(norm_gain, inner)).astype(bf16)
 
     for j in range(1, n_f):
-        for n in range(2):
-            out_copy(j, lax.rem(f + n_f - j, n_f), n).wait_recv()
+        out_copy(j, lax.rem(f + n_f - j, n_f)).wait_recv()
     width = wo_inner.shape[1]
     for w in range(n_f):
         part[:, w * width : (w + 1) * width] = (
@@ -462,8 +492,7 @@
     for i in range(1, n_t):
         last_copy(i).start()
     for j in range(1, n_f):
-        for n in range(2):
-            out_copy(j, f, n).wait_send()
+        out_copy(j, f).wait_send()
     for g in range(groups):
 
         @pl.when(s + 1 < n_s)
@@ -478,7 +507,7 @@
     for i in range(1, n_t):
         last_copy(i).wait_recv()
         acc = acc + peer[i - 1].astype(f32)
-    result[...] = acc.astype(bf16)
+    result[0] = acc.astype(bf16)
     for i in range(1, n_t):
         last_copy(i).wait_send()
 
@@ -488,7 +517,6 @@
     rate_log, decay_extra, norm_gain, pool_mix, pool_gain, w_out_inner, w_out_pool,
 ):
     n_s, n_f, n_t = sizes
-    tp_rank = lax.axis_index("tp")
     tok = tokens[0]
     rows, half_d = tok.shape
     ks, inner = w_inner.shape
@@ -501,14 +529,7 @@
     hw = total // n_f // NH
     d = half_d * n_t
 
-    def mine(array, axis):
-        size = array.shape[axis] // n_t
-        return lax.dynamic_slice_in_dim(array, tp_rank * size, size, axis)
-
-    step_w = mine(w_step, 2).reshape(d, 2 * heads)
-    taps = jnp.concatenate(
-        [mine(conv_inner, 1), mine(conv_cross[:, 0], 1), mine(conv_cross[:, 1], 1)], axis=1
-    ).astype(f32)
+    step_w = w_step.reshape(d, 2 * heads * n_t)
     vmem = pl.BlockSpec(memory_space=pltpu.VMEM)
     dma = pltpu.SemaphoreType.DMA
 
@@ -524,9 +545,10 @@
             shape(RIM, stream),
             shape(rows, pool),
             shape(rows, pool),
+            shape(n_f, *w_out_pool.shape),
         ),
-        in_specs=[vmem] * 7,
-        out_specs=(vmem,) * 6,
+        in_specs=[vmem] * 8,
+        out_specs=(vmem,) * 7,
         scratch_shapes=[
             pltpu.VMEM((ks, total), bf16),
             pltpu.VMEM((NH, d, hw), bf16),
@@ -535,21 +557,20 @@
             dma((NH, n_s)), dma((NH, n_s)), dma((NH, n_s)), dma((NH, n_s)),
             dma((n_f,)), dma((n_f,)), dma((n_f, n_t)), dma((n_f, n_t)),
             dma((NH, n_f - 1)), dma((NH, n_f - 1)), dma((4,)), dma((4,)),
+            dma((n_f,)), dma((n_f,)),
         ],
         compiler_params=pltpu.CompilerParams(collective_id=0, has_side_effects=True),
-    )(tok, w_inner, w_write, w_read, w_gate, w_pool_in, step_w)
+    )(tok, w_inner, w_write, w_read, w_gate, w_pool_in, step_w, w_out_pool)
 
     result = pl.pallas_call(
         functools.partial(mixer_kernel, sizes),
-        out_shape=shape(rows // n_t, d),
-        in_specs=[vmem] * 14,
-        out_specs=vmem,
+        out_shape=shape(1, rows // n_t, d),
+        in_specs=[vmem] * 15,
         scratch_shapes=[
             pltpu.VMEM((rows + 16, stream), f32),
             pltpu.VMEM((rows, stream), bf16),
             pltpu.VMEM((rows, inner), f32),
             pltpu.VMEM((n_f,) + w_out_inner.shape, bf16),
-            pltpu.VMEM((n_f,) + w_out_pool.shape, bf16),
             pltpu.VMEM((groups, STATE, inner // groups), f32),
             pltpu.VMEM((groups, STATE, inner // groups), f32),
             pltpu.VMEM((groups, STATE, inner // groups), bf16),
@@ -559,22 +580,22 @@
             pltpu.VMEM((rows, d), bf16),
             pltpu.VMEM((n_t - 1, rows // n_t, d), bf16),
             pltpu.VMEM((rows, pool), bf16),
-            dma((n_f, 2)), dma((n_f, 2)), dma((groups,)), dma((groups,)),
+            dma((n_f,)), dma((n_f,)), dma((groups,)), dma((groups,)),
             dma((groups,)), dma((groups,)), dma((n_t - 1,)), dma((n_t - 1,)),
         ],
         compiler_params=pltpu.CompilerParams(collective_id=1, has_side_effects=True),
     )(
         *moved,
         decay_extra[0].reshape(rows, 2 * heads),
-        mine(rate_log, 1).reshape(1, 2 * heads),
-        taps,
-        mine(norm_gain, 0)[None],
-        mine(pool_mix, 0),
-        mine(pool_gain, 0)[None],
+        rate_log,
+        conv_inner,
+        conv_cross.reshape(CONV, -1),
+        norm_gain[None],
+        pool_mix,
+        pool_gain[None],
         w_out_inner,
-        w_out_pool,
     )
-    return result[None]
+    return result
 
 
 def solution(mesh):

time: 106 us -> 88.6 us (0.84)
  Pallas kernels: 96.4 us -> 83.2 us
  local copies, waits for them, and re-layouts: 8.34 us -> 4.79 us
    pallas_call x1, Pallas kernels: 50.4 us -> 33.2 us  [body(): pl.pallas_call(functools.partial(mixer_kernel, sizes), out_shape=shape(1,...]
    pallas_call x1, Pallas kernels: 46 us -> 50 us  [body(): pl.pallas_call(functools.partial(project_kernel, sizes), out_shape=(shape...]
    dynamic_slice x7 -> x0, local copies, waits for them, and re-layouts: 3.65 us -> none  [mine(): return lax.dynamic_slice_in_dim(array, tp_rank * size, size, axis)]
    unnamed x13 -> x6, local copies, waits for them, and re-layouts: 1.7 us -> 2.28 us
where the time goes in v1:
time: 88.6 us; the launch traced here: 88 us
  Pallas kernels  83.2 us (94%)
  local copies, waits for them, and re-layouts  4.79 us (5%)
    pallas_call x1, Pallas kernels, body(): pl.pallas_call(functools.partial(project_kernel, sizes), out_shape=(shape...  50 us
    pallas_call x1, Pallas kernels, body(): pl.pallas_call(functools.partial(mixer_kernel, sizes), out_shape=shape(1,...  33.2 us
    unnamed x6, local copies, waits for them, and re-layouts  2.28 us

profile of v1, /device:TPU:9, one launch (start us, length us, event | category | flops | bytes accessed | tf_op | source)
XLA Modules:
  0.0 88.0 jit_solution(2726410005648656087)
XLA Ops:
  0.0 0.0 copy-start
  0.0 0.0 copy-start.1
  0.0 1.8 %copy.19.w_step = bf16[1024,64]{1,0:T(8,128)(2,1)} copy(bf16[1024,64]{0,1:T(8,128)(2,1)} %bitcast.8) | data formatting | bytes 262144 | tf_op jit(solution)/shard_map/reshape | solution.py:532
  1.8 50.0 %shard_map.154 = (bf16[256,3072]{1,0:T(8,128)(2,1)}, f32[256,32]{1,0:T(8,128)}, bf16[16,1536]{1,0:T(8,128)(2,1)}, bf16[16,1536]{1,0:T(8,128)(2,1)}, bf16[256,512...) custom-call(bf16[256,512]{1,0:T(8,128)(2,1)} %bitcast.7, bf16[256,1024]{1,0:T(8,128)(2,1)} %w_inner.1, ...), custom_call_target="tpu_custom_call" | custom-call | tf_op jit(solution)/shard_map/pallas_call | solution.py:539
  51.8 0.0 copy-done
  51.8 0.8 copy.20.extra
  52.5 0.0 copy-done.1
  52.5 0.6 copy.21
  53.1 33.2 %shard_map.155 = bf16[1,128,1024]{2,1,0:T(8,128)(2,1)} custom-call(bf16[256,3072]{1,0:T(8,128)(2,1)} %get-tuple-element.12.proj, f32[256,32]{1,0:T(8,128)} %get-tuple-element.13.raw, bf16[16,1536]{1,0:T(8,128)(2,1)} %get-tuple-element.14.rim_lo, bf16[16,1536]{1,0:T(8,128)(2,1)} %get-tuple-element.15.rim_hi, bf16[256,512]{1,0:T(8,128)(2,1)} %get-tuple-element.16.pool_lo, ...), custom_call_target="tpu_custom_call" | custom-call | tf_op jit(solution)/shard_map/pallas_call | solution.py:565
  86.3 1.7 %copy.23 = bf16[1,128,1024]{2,1,0:T(8,128)(2,1)} copy(bf16[1,128,1024]{2,1,0:T(8,128)(2,1)} %shard_map.155) | data formatting | bytes 524288
Async XLA Ops:
  0.0 51.8 %copy-start = (f32[1,256,2,16]{1,3,2,0:T(8,128)S(1)}, f32[1,256,2,16]{1,3,2,0:T(8,128)}, u32[]{:S(2)}) copy-start(f32[1,256,2,16]{1,3,2,0:T(8,128)} %param.26) | copy-start | bytes 98308
  0.0 52.5 %copy-start.1 = (bf16[5,2,512]{2,1,0:T(2,128)(2,1)S(1)}, bf16[5,2,512]{2,1,0:T(2,128)(2,1)}, u32[]{:S(2)}) copy-start(bf16[5,2,512]{2,1,0:T(2,128)(2,1)} %param.24) | copy-start | bytes 30724
